TPU v7x, 512 devices: a whole 4x4x16 slice. The times are simulated.
512 devices in a mesh: fs: 32 (over z, core), tp: 16 (over y, x).
Axes of the slice: x: 4, y: 4, z: 16, core: 2. Of those that a mesh axis runs over, the one named last changes fastest.
Arguments:
- late_input: bfloat16 [4096, 2048], P('fs'), may hold values from -6 to 6
- early_input: bfloat16 [4096, 2048], P('fs'), may hold values from -6 to 6
- early_mid: bfloat16 [4096, 2048], P('fs'), may hold values from -6 to 6
- cotangent: bfloat16 [4096, 2048], P('fs'), may hold values from -6 to 6
- gain_first: float32 [2048], replicated, may hold values from 0.1 to 1.9
- gain_second: float32 [2048], replicated, may hold values from 0.1 to 1.9
- gate_first: bfloat16 [2048, 2816], P('fs', 'tp'), may hold values from -0.125 to 0.125
- up_first: bfloat16 [2048, 2816], P('fs', 'tp'), may hold values from -0.125 to 0.125
- down_first: bfloat16 [2816, 2048], P('tp', 'fs'), may hold values from -0.109375 to 0.109375
- gate_second: bfloat16 [2048, 2816], P('fs', 'tp'), may hold values from -0.125 to 0.125
- up_second: bfloat16 [2048, 2816], P('fs', 'tp'), may hold values from -0.125 to 0.125
- down_second: bfloat16 [2816, 2048], P('tp', 'fs'), may hold values from -0.109375 to 0.109375
- sum_gate_first: float32 [2048, 2816], P('fs', 'tp'), may hold values from -256 to 256
- sum_up_first: float32 [2048, 2816], P('fs', 'tp'), may hold values from -256 to 256
- sum_down_first: float32 [2816, 2048], P('tp', 'fs'), may hold values from -256 to 256
- sum_gate_second: float32 [2048, 2816], P('fs', 'tp'), may hold values from -256 to 256
- sum_up_second: float32 [2048, 2816], P('fs', 'tp'), may hold values from -256 to 256
- sum_down_second: float32 [2816, 2048], P('tp', 'fs'), may hold values from -256 to 256
Outputs:
- late_mid: bfloat16 [4096, 2048], P('fs')
- late_out: bfloat16 [4096, 2048], P('fs')
- input_grad: bfloat16 [4096, 2048], P('fs')
- new_gate_first: float32 [2048, 2816], P('fs', 'tp')
- new_up_first: float32 [2048, 2816], P('fs', 'tp')
- new_down_first: float32 [2816, 2048], P('tp', 'fs')
- new_gate_second: float32 [2048, 2816], P('fs', 'tp')
- new_up_second: float32 [2048, 2816], P('fs', 'tp')
- new_down_second: float32 [2816, 2048], P('tp', 'fs')
All inputs are finite; a program needn't handle non-finite values.
Results may differ from a plain program's by a relative error of at most 0.015.
Values may be sent and summed in bfloat16 or wider, within the bound.
No kernel may reach another device: no remote copies, remote signals or barrier semaphores. Data moves between devices by JAX's collectives and lax.ppermute only.
A program may use at most 128 MiB of HBM per device.

v0:
```python
import jax
import jax.numpy as jnp
from jax import lax
from jax.sharding import PartitionSpec as P

norm_eps = 1e-06


def sent_together(arrays, axis, dim, along):
    both = jnp.concatenate(arrays, axis=along)
    whole, at, outs = (lax.all_gather(both, axis, axis=dim, tiled=True), 0, [])
    for a in arrays:
        outs.append(lax.slice_in_dim(whole, at, at + a.shape[along], axis=along))
        at += a.shape[along]
    return tuple(outs)


def gather_turned(arrays, axis, dims):
    turned = [jnp.moveaxis(a, dim, 0) for a, dim in zip(arrays, dims)]
    widths = [t[0].size for t in turned]
    both = jnp.concatenate([t.reshape(-1, w) for t, w in zip(turned, widths)], axis=1)
    whole = lax.all_gather(both, axis, axis=0, tiled=True)
    blocks = jnp.split(whole, [sum(widths[:k]) for k in range(1, len(widths))], axis=1)
    return tuple(
        (
            jnp.moveaxis(b.reshape(-1, *t.shape[1:]), 0, dim)
            for b, t, dim in zip(blocks, turned, dims)
        )
    )


def normalize(values, gain_vector):
    widened = values.astype(jnp.float32)
    factor = lax.rsqrt(jnp.mean(widened * widened, axis=-1, keepdims=True) + norm_eps)
    normed = (widened * factor * gain_vector).astype(jnp.bfloat16)
    return (widened, factor, normed)


def block_forward(values, params):
    gain_vector, w_gate, w_up, w_down = params
    widened, factor, normed = normalize(values, gain_vector)
    gate_pre = jnp.dot(normed, w_gate, preferred_element_type=jnp.float32)
    up_pre = jnp.dot(normed, w_up, preferred_element_type=jnp.float32)
    hidden = (jax.nn.silu(gate_pre) * up_pre).astype(jnp.bfloat16)
    branch = lax.psum(
        jnp.dot(hidden, w_down, preferred_element_type=jnp.float32).astype(jnp.bfloat16), "tp"
    ).astype(jnp.float32)
    return (widened + 0.5 * branch).astype(jnp.bfloat16)


def block_backward(values, cotangent, params):
    gain_vector, w_gate, w_up, w_down = params
    widened, factor, normed = normalize(values, gain_vector)
    gate_pre = jnp.dot(normed, w_gate, preferred_element_type=jnp.float32)
    up_pre = jnp.dot(normed, w_up, preferred_element_type=jnp.float32)
    sigmoid_gate = jax.nn.sigmoid(gate_pre)
    activated = gate_pre * sigmoid_gate
    hidden = (activated * up_pre).astype(jnp.bfloat16)
    hidden_grad = 0.5 * jnp.einsum(
        "td,fd->tf", cotangent, w_down, preferred_element_type=jnp.float32
    )
    gate_grad = (
        hidden_grad * up_pre * sigmoid_gate * (1.0 + gate_pre * (1.0 - sigmoid_gate))
    ).astype(jnp.bfloat16)
    up_grad = (hidden_grad * activated).astype(jnp.bfloat16)
    partial_value = jnp.einsum("tf,df->td", gate_grad, w_gate, preferred_element_type=jnp.float32)
    partial_value = partial_value + jnp.einsum(
        "tf,df->td", up_grad, w_up, preferred_element_type=jnp.float32
    )
    normed_grad = lax.psum(partial_value.astype(jnp.bfloat16), "tp").astype(jnp.float32)
    scaled = normed_grad * gain_vector
    unit_rows = widened * factor
    rows_grad = cotangent.astype(jnp.float32) + factor * (
        scaled - unit_rows * jnp.mean(scaled * unit_rows, axis=-1, keepdims=True)
    )
    return (rows_grad, (normed, cotangent, gate_grad, up_grad, hidden))


def fold_pair(pieces, columns_in):
    return (
        jnp.einsum("td,tf->df", columns_in, pieces[0], preferred_element_type=jnp.float32),
        jnp.einsum("td,tf->df", columns_in, pieces[1], preferred_element_type=jnp.float32),
    )


def fold_block(pieces, columns_in, columns_out):
    paired = fold_pair(pieces[0:2], columns_in)
    return paired + (
        jnp.einsum("tf,td->fd", pieces[2], columns_out, preferred_element_type=jnp.float32),
    )


def per_device(
    late_input,
    early_input,
    early_mid,
    cotangent,
    gain_first,
    gain_second,
    gate_first,
    up_first,
    down_first,
    gate_second,
    up_second,
    down_second,
    sum_gate_first,
    sum_up_first,
    sum_down_first,
    sum_gate_second,
    sum_up_second,
    sum_down_second,
):
    rows_in = sent_together((gate_first, up_first, gate_second, up_second), "fs", 0, 1)
    cols_out = gather_turned((down_first, down_second), "fs", (1, 1))
    first_params = (gain_first, rows_in[0], rows_in[1], cols_out[0])
    second_params = (gain_second, rows_in[2], rows_in[3], cols_out[1])
    late_mid = block_forward(late_input, first_params)
    late_out = block_forward(late_mid, second_params)
    mid_grad, saved_second = block_backward(early_mid, cotangent, second_params)
    mid_grad = mid_grad.astype(jnp.bfloat16)
    rows_grad, saved_first = block_backward(early_input, mid_grad, first_params)
    pieces = sent_together(
        (
            saved_second[2],
            saved_second[3],
            saved_second[4],
            saved_first[2],
            saved_first[3],
            saved_first[4],
        ),
        "fs",
        0,
        1,
    )
    upper = fold_block(
        pieces[0:3],
        lax.all_to_all(saved_second[0], "fs", split_axis=1, concat_axis=0, tiled=True),
        lax.all_to_all(saved_second[1], "fs", split_axis=1, concat_axis=0, tiled=True),
    )
    lower = fold_block(
        pieces[3:6],
        lax.all_to_all(saved_first[0], "fs", split_axis=1, concat_axis=0, tiled=True),
        lax.all_to_all(saved_first[1], "fs", split_axis=1, concat_axis=0, tiled=True),
    )
    result = upper + lower
    grads_second = (result[0], result[1], 0.5 * result[2])
    grads_first = (result[3], result[4], 0.5 * result[5])
    return (
        late_mid,
        late_out,
        rows_grad.astype(jnp.bfloat16),
        sum_gate_first + grads_first[0],
        sum_up_first + grads_first[1],
        sum_down_first + grads_first[2],
        sum_gate_second + grads_second[0],
        sum_up_second + grads_second[1],
        sum_down_second + grads_second[2],
    )


def solution(mesh):
    in_specs = (
        P("fs", None),
        P("fs", None),
        P("fs", None),
        P("fs", None),
        P(),
        P(),
        P("fs", "tp"),
        P("fs", "tp"),
        P("tp", "fs"),
        P("fs", "tp"),
        P("fs", "tp"),
        P("tp", "fs"),
        P("fs", "tp"),
        P("fs", "tp"),
        P("tp", "fs"),
        P("fs", "tp"),
        P("fs", "tp"),
        P("tp", "fs"),
    )
    out_specs = (
        P("fs", None),
        P("fs", None),
        P("fs", None),
        P("fs", "tp"),
        P("fs", "tp"),
        P("tp", "fs"),
        P("fs", "tp"),
        P("fs", "tp"),
        P("tp", "fs"),
    )
    return jax.shard_map(
        per_device, mesh=mesh, in_specs=in_specs, out_specs=out_specs, check_vma=False
    )
```

profile of v0, /device:TPU:1, one launch (start us, length us, event | category | flops | bytes accessed | tf_op | source)
XLA Modules:
  0.0 560.9 jit_solution(5887314163387625684)
XLA Ops:
  8.8 1.6 pad_maximum_fusion
  14.1 2.0 fusion.47
  16.1 71.3 %all-gather.6.cloned.1.call-done = bf16[2048,352]{1,0:T(8,128)(2,1)} async-done(((bf16[64,352]{1,0:T(8,128)(2,1)}), bf16[2048,352]{1,0:T(8,128)(2,1)}) %all-gather.6.cloned.1.call-update) | async-done | bytes 1441808 | tf_op jit(solution)/shard_map/all_gather | solution.py:22
  87.5 2.1 fusion.20
  89.6 70.4 %all-gather.4.cloned.1.call-done = bf16[2048,704]{1,0:T(8,128)(2,1)} async-done(((bf16[64,704]{1,0:T(8,128)(2,1)}), bf16[2048,704]{1,0:T(8,128)(2,1)}) %all-gather.4.cloned.1.call-update) | async-done | bytes 2883600 | tf_op jit(solution)/shard_map/all_gather | solution.py:11
  160.0 2.6 fusion.74
  162.6 3.2 constant_dynamic-update-slice_fusion.3
  166.5 1.6 fusion.93
  168.1 3.9 convolution_convert_fusion.1
  177.5 110.1 %all-reduce.7.cloned.1.call-done = (bf16[128,2048]{1,0:T(8,128)(2,1)}, bf16[128,2048]{1,0:T(8,128)(2,1)}) async-done(((bf16[128,2048]{1,0:T(8,128)(2,1)}, bf16[128,2048]{1,0:T(8,128)(2,1)}), (bf16[128,2048]{1,0:T(8,128)(2,1)}, bf16[128,2048]{1,0:T(8,128)(2,1)})) %all-reduce.7.cloned.1.call-update) | async-done | bytes 1048592 | tf_op jit(solution)/shard_map/psum | solution.py:45
  287.6 1.7 fusion.65
  289.3 1.7 fusion.48
  291.0 1.8 fusion.52
  295.9 1.7 fusion.82
  297.6 4.0 convolution_convert_fusion
  304.3 2.1 copy.27
  306.4 14.7 %all-to-all-start = ((bf16[128,32,64]{0,2,1:T(8,128)(2,1)}), bf16[128,32,64]{0,2,1:T(8,128)(2,1)S(1)}, u32[]{:S(2)}, u32[]{:S(2)}) async-start(bf16[128,32,64]{0,2,1:T(8,128)(2,1)} %bitcast.3), calls=%async_computation | async-start | bytes 1048576 | tf_op jit(solution)/shard_map/all_to_all | solution.py:142
  322.2 32.5 %all-to-all-done = bf16[128,32,64]{0,2,1:T(8,128)(2,1)S(1)} async-done(((bf16[128,32,64]{0,2,1:T(8,128)(2,1)}), bf16[128,32,64]{0,2,1:T(8,128)(2,1)S(1)}, u32[]{:S(2)}, u32[]{:S(2)}) %all-to-all-start) | async-done | bytes 524320 | tf_op jit(solution)/shard_map/all_to_all | solution.py:142
  354.6 4.2 all-to-all-start.2
  359.8 32.5 %all-to-all-done.2 = bf16[128,32,64]{0,2,1:T(8,128)(2,1)S(1)} async-done(((bf16[128,32,64]{0,2,1:T(8,128)(2,1)}), bf16[128,32,64]{0,2,1:T(8,128)(2,1)S(1)}, u32[]{:S(2)}, u32[]{:S(2)}) %all-to-all-start.2) | async-done | bytes 524320 | tf_op jit(solution)/shard_map/all_to_all | solution.py:137
  392.3 5.0 all-to-all-start.1
  398.4 22.9 %all-reduce.5.cloned.1.call-done = (bf16[128,2048]{1,0:T(8,128)(2,1)}, bf16[128,2048]{1,0:T(8,128)(2,1)}) async-done(((bf16[128,2048]{1,0:T(8,128)(2,1)}, bf16[128,2048]{1,0:T(8,128)(2,1)}), (bf16[128,2048]{1,0:T(8,128)(2,1)}, bf16[128,2048]{1,0:T(8,128)(2,1)})) %all-reduce.5.cloned.1.call-update) | async-done | bytes 1048592 | tf_op jit(solution)/shard_map/psum | solution.py:45
  422.6 8.3 %all-to-all-done.1 = bf16[128,32,64]{0,2,1:T(8,128)(2,1)} async-done(((bf16[128,32,64]{0,2,1:T(8,128)(2,1)}), bf16[128,32,64]{0,2,1:T(8,128)(2,1)}, u32[]{:S(2)}, u32[]{:S(2)}) %all-to-all-start.1) | async-done | bytes 524320 | tf_op jit(solution)/shard_map/all_to_all | solution.py:143
  430.9 6.1 %all-to-all-start.3 = ((bf16[128,32,64]{0,2,1:T(8,128)(2,1)}), bf16[128,32,64]{0,2,1:T(8,128)(2,1)S(1)}, u32[]{:S(2)}, u32[]{:S(2)}) async-start(bf16[128,32,64]{0,2,1:T(8,128)(2,1)} %bitcast.9), calls=%async_computation.3 | async-start | bytes 1048576 | tf_op jit(solution)/shard_map/all_to_all | solution.py:138
  437.1 2.7 fusion.59
  439.8 98.8 %all-gather.8.cloned.1.call-done = bf16[4096,1056]{0,1:T(8,128)(2,1)} async-done(((bf16[128,1056]{0,1:T(8,128)(2,1)}), bf16[4096,1056]{0,1:T(8,128)(2,1)}) %all-gather.8.cloned.1.call-update) | async-done | bytes 8650768 | tf_op jit(solution)/shard_map/all_gather | solution.py:11
  538.7 2.6 fusion.23
  541.2 2.6 fusion.26
  543.9 2.6 fusion.35
  546.4 2.6 fusion.38
  549.1 2.7 fusion.32
  551.8 2.6 fusion.44
  (75 shorter events, 21.7 us)
Async XLA Ops:
  7.2 80.3 %all-gather.6.cloned.1.call-start = ((), (), s32[]{:S(2)}) async-start(), calls=%async_computation.5 | async-start | bytes 1622016 | tf_op jit(solution)/shard_map/all_gather | solution.py:22
  8.7 151.3 %all-gather.4.cloned.1.call-start = ((), (), s32[]{:S(2)}) async-start(), calls=%async_computation.4 | async-start | bytes 3244032 | tf_op jit(solution)/shard_map/all_gather | solution.py:11
  10.4 277.2 %all-reduce.7.cloned.1.call-start = ((), (), s32[]{:S(2)}) async-start(), calls=%async_computation.8 | async-start | bytes 2097152 | tf_op jit(solution)/shard_map/psum | solution.py:45
  16.1 150.4 %copy-start.12 = (f32[2048]{0:T(1024)S(1)}, f32[2048]{0:T(1024)}, u32[]{:S(2)}) copy-start(f32[2048]{0:T(1024)} %param.22) | copy-start | bytes 24580
  160.0 6.5 %copy-start = (bf16[2048,704]{1,0:T(8,128)(2,1)S(1)}, bf16[2048,704]{1,0:T(8,128)(2,1)}, u32[]{:S(2)}) copy-start(bf16[2048,704]{1,0:T(8,128)(2,1)} %all-gather.4.cloned.1.call-done) | copy-start | bytes 8650756
  174.1 115.2 %copy-start.11 = (f32[2048]{0:T(1024)S(1)}, f32[2048]{0:T(1024)}, u32[]{:S(2)}) copy-start(f32[2048]{0:T(1024)} %param.23) | copy-start | bytes 24580
  174.1 247.1 %all-reduce.5.cloned.1.call-start = ((), (), s32[]{:S(2)}) async-start(), calls=%async_computation.7 | async-start | bytes 2097152 | tf_op jit(solution)/shard_map/psum | solution.py:45
  175.6 0.9 copy-start.5
  287.6 6.0 %copy-start.10 = (bf16[2048,352]{1,0:T(8,128)(2,1)S(1)}, bf16[2048,352]{1,0:T(8,128)(2,1)}, u32[]{:S(2)}) copy-start(bf16[2048,352]{1,0:T(8,128)(2,1)} %all-gather.6.cloned.1.call-done) | copy-start | bytes 4325380
  287.6 6.5 %copy-start.6 = (bf16[128,2048]{1,0:T(8,128)(2,1)S(1)}, bf16[128,2048]{1,0:T(8,128)(2,1)}, u32[]{:S(2)}) copy-start(bf16[128,2048]{1,0:T(8,128)(2,1)} %copy-done.5) | copy-start | bytes 1572868
  289.2 6.6 %copy-start.8 = (bf16[128,2048]{1,0:T(8,128)(2,1)}, bf16[128,2048]{1,0:T(8,128)(2,1)S(1)}, u32[]{:S(2)}) copy-start(bf16[128,2048]{1,0:T(8,128)(2,1)S(1)} %get-tuple-element.22) | copy-start | bytes 1572868
  292.8 0.8 copy-start.2
  303.5 17.6 %copy-start.4 = (bf16[128,2048]{1,0:T(8,128)(2,1)S(1)}, bf16[128,2048]{1,0:T(8,128)(2,1)}, u32[]{:S(2)}) copy-start(bf16[128,2048]{1,0:T(8,128)(2,1)} %fusion.47) | copy-start | bytes 1572868
  303.5 55.3 %copy-start.3 = (bf16[128,2048]{1,0:T(8,128)(2,1)S(1)}, bf16[128,2048]{1,0:T(8,128)(2,1)}, u32[]{:S(2)}) copy-start(bf16[128,2048]{1,0:T(8,128)(2,1)} %copy-done.2) | copy-start | bytes 1572868
  303.6 235.1 %all-gather.8.cloned.1.call-start = ((), (), s32[]{:S(2)}) async-start(), calls=%async_computation.6 | async-start | bytes 8921088 | tf_op jit(solution)/shard_map/all_gather | solution.py:11
  304.3 93.1 %copy-start.7 = (bf16[128,2048]{1,0:T(8,128)(2,1)S(1)}, bf16[128,2048]{1,0:T(8,128)(2,1)}, u32[]{:S(2)}) copy-start(bf16[128,2048]{1,0:T(8,128)(2,1)} %param.21) | copy-start | bytes 1572868
  306.4 114.8 %copy-start.1 = (bf16[128,2048]{1,0:T(8,128)(2,1)S(1)}, bf16[128,2048]{1,0:T(8,128)(2,1)}, u32[]{:S(2)}) copy-start(bf16[128,2048]{1,0:T(8,128)(2,1)} %param.19) | copy-start | bytes 1572868
  306.4 48.2 %all-to-all-start = ((bf16[128,32,64]{0,2,1:T(8,128)(2,1)}), bf16[128,32,64]{0,2,1:T(8,128)(2,1)S(1)}, u32[]{:S(2)}, u32[]{:S(2)}) async-start(bf16[128,32,64]{0,2,1:T(8,128)(2,1)} %bitcast.3), calls=%async_computation | async-start | bytes 1048576 | tf_op jit(solution)/shard_map/all_to_all | solution.py:142
  354.6 82.4 %copy-start.9 = (bf16[128,2048]{1,0:T(8,128)(2,1)S(1)}, bf16[128,2048]{1,0:T(8,128)(2,1)}, u32[]{:S(2)}) copy-start(bf16[128,2048]{1,0:T(8,128)(2,1)} %copy-done.8) | copy-start | bytes 1572868
  354.6 37.7 %all-to-all-start.2 = ((bf16[128,32,64]{0,2,1:T(8,128)(2,1)}), bf16[128,32,64]{0,2,1:T(8,128)(2,1)S(1)}, u32[]{:S(2)}, u32[]{:S(2)}) async-start(bf16[128,32,64]{0,2,1:T(8,128)(2,1)} %bitcast.7), calls=%async_computation.2 | async-start | bytes 1048576 | tf_op jit(solution)/shard_map/all_to_all | solution.py:137
  392.3 38.6 %all-to-all-start.1 = ((bf16[128,32,64]{0,2,1:T(8,128)(2,1)}), bf16[128,32,64]{0,2,1:T(8,128)(2,1)}, u32[]{:S(2)}, u32[]{:S(2)}) async-start(bf16[128,32,64]{0,2,1:T(8,128)(2,1)} %bitcast.5), calls=%async_computation.1 | async-start | bytes 1048576 | tf_op jit(solution)/shard_map/all_to_all | solution.py:143
  398.4 140.3 %copy-start.13 = (f32[64,176]{1,0:T(8,128)S(1)}, f32[64,176]{1,0:T(8,128)}, u32[]{:S(2)}) copy-start(f32[64,176]{1,0:T(8,128)} %param.30) | copy-start | bytes 135172
  430.9 120.8 %all-to-all-start.3 = ((bf16[128,32,64]{0,2,1:T(8,128)(2,1)}), bf16[128,32,64]{0,2,1:T(8,128)(2,1)S(1)}, u32[]{:S(2)}, u32[]{:S(2)}) async-start(bf16[128,32,64]{0,2,1:T(8,128)(2,1)} %bitcast.9), calls=%async_computation.3 | async-start | bytes 1048576 | tf_op jit(solution)/shard_map/all_to_all | solution.py:138
  437.0 104.2 %copy-start.14 = (f32[64,176]{1,0:T(8,128)S(1)}, f32[64,176]{1,0:T(8,128)}, u32[]{:S(2)}) copy-start(f32[64,176]{1,0:T(8,128)} %param.31) | copy-start | bytes 135172
  439.8 104.0 %copy-start.15 = (f32[64,176]{1,0:T(8,128)S(1)}, f32[64,176]{1,0:T(8,128)}, u32[]{:S(2)}) copy-start(f32[64,176]{1,0:T(8,128)} %param.33) | copy-start | bytes 135172
  439.8 106.6 %copy-start.16 = (f32[64,176]{1,0:T(8,128)S(1)}, f32[64,176]{1,0:T(8,128)}, u32[]{:S(2)}) copy-start(f32[64,176]{1,0:T(8,128)} %param.34) | copy-start | bytes 135172
  541.2 7.8 %copy-start.17 = (f32[176,64]{0,1:T(8,128)S(1)}, f32[176,64]{0,1:T(8,128)}, u32[]{:S(2)}) copy-start(f32[176,64]{0,1:T(8,128)} %param.32) | copy-start | bytes 135172
  546.4 5.3 copy-start.18
Sparse Core Ops, SparseCore 0:
  10.7 76.7 all-gather.5
  90.1 69.8 all-gather.3
  174.2 113.2 all-reduce.6
  303.7 117.5 all-reduce.4
  423.1 115.4 all-gather.7
where the time goes:
time: 562 us; the launch traced here: 561 us
  waiting for transfers between devices  447 us (80%)
  matrix products  41.5 us (7%)
  starting transfers between devices  30.4 us (5%)
  other arithmetic  22 us (4%)
  between operations  14 us (2%)
  local copies, waits for them, and re-layouts  6.1 us (1%)
    all_gather x2, waiting for transfers between devices, sent_together(): whole, at, outs = (lax.all_gather(both, axis, axis=dim, tiled=True), 0, [])  169 us
    psum x2, waiting for transfers between devices, block_forward(): lax.psum(jnp.dot(hidden, w_down, preferred_element_type=jnp.float32).asty...  133 us
    all_gather x1, waiting for transfers between devices, gather_turned(): whole = lax.all_gather(both, axis, axis=0, tiled=True)  71.3 us
    all_to_all x1, waiting for transfers between devices, per_device(): lax.all_to_all(saved_second[0], 'fs', split_axis=1, concat_axis=0, tiled=...  32.5 us
    all_to_all x1, waiting for transfers between devices, per_device(): lax.all_to_all(saved_first[0], 'fs', split_axis=1, concat_axis=0, tiled=T...  32.5 us
    all_to_all x1, starting transfers between devices, per_device(): lax.all_to_all(saved_first[0], 'fs', split_axis=1, concat_axis=0, tiled=T...  14.7 us
  transfers between devices with their start and end apart: 9, of which 8 were waited for; matrix products, arithmetic and copies ran while one was open for 6% of the time, Pallas kernels for 0%

commit v1 on v0

--- a/solution.py
+++ b/solution.py
@@ -134,7 +134,15 @@
     )
     upper = fold_block(
         pieces[0:3],
-        lax.all_to_all(saved_second[0], "fs", split_axis=1, concat_axis=0, tiled=True),
+        jnp.concatenate(
+            jax.lax.all_to_all(
+                jnp.stack(jnp.split(saved_second[0], jax.lax.axis_size("fs"), axis=1)),
+                axis_name="fs",
+                split_axis=0,
+                concat_axis=0,
+            ),
+            axis=0,
+        ),
         lax.all_to_all(saved_second[1], "fs", split_axis=1, concat_axis=0, tiled=True),
     )
     lower = fold_block(

time: 562 us -> 562 us (level)
  transfers between devices with their start and end apart: 9 -> 9, of which waited for: 8 -> 8; matrix products, arithmetic and copies ran while one was open for 6% -> 7% of each run, Pallas kernels for 0% -> 0%
where the time goes in v1:
time: 562 us; the launch traced here: 561 us
  waiting for transfers between devices  445 us (79%)
  matrix products  41.7 us (7%)
  starting transfers between devices  30.4 us (5%)
  other arithmetic  22 us (4%)
  between operations  14.2 us (3%)
  local copies, waits for them, and re-layouts  7.94 us (1%)
    all_gather x2, waiting for transfers between devices, sent_together(): whole, at, outs = (lax.all_gather(both, axis, axis=dim, tiled=True), 0, [])  169 us
    psum x2, waiting for transfers between devices, block_forward(): lax.psum(jnp.dot(hidden, w_down, preferred_element_type=jnp.float32).asty...  134 us
    all_gather x1, waiting for transfers between devices, gather_turned(): whole = lax.all_gather(both, axis, axis=0, tiled=True)  71.3 us
    all_to_all x1, waiting for transfers between devices, per_device(): jax.lax.all_to_all(jnp.stack(jnp.split(saved_second[0], jax.lax.axis_size...  32.5 us
    all_to_all x1, waiting for transfers between devices, per_device(): lax.all_to_all(saved_first[0], 'fs', split_axis=1, concat_axis=0, tiled=T...  30.5 us
    all_to_all x1, starting transfers between devices, per_device(): lax.all_to_all(saved_first[0], 'fs', split_axis=1, concat_axis=0, tiled=T...  14.7 us
  transfers between devices with their start and end apart: 9, of which 8 were waited for; matrix products, arithmetic and copies ran while one was open for 7% of the time, Pallas kernels for 0%

profile of v1, /device:TPU:1, one launch (start us, length us, event | category | flops | bytes accessed | tf_op | source)
XLA Modules:
  0.0 561.1 jit_solution(13184744212215624590)
XLA Ops:
  8.8 1.6 pad_maximum_fusion
  14.1 2.0 fusion.47
  16.1 71.3 %all-gather.6.cloned.1.call-done = bf16[2048,352]{1,0:T(8,128)(2,1)} async-done(((bf16[64,352]{1,0:T(8,128)(2,1)}), bf16[2048,352]{1,0:T(8,128)(2,1)}) %all-gather.6.cloned.1.call-update) | async-done | bytes 1441808 | tf_op jit(solution)/shard_map/all_gather | solution.py:22
  87.5 2.1 fusion.20
  89.6 70.4 %all-gather.4.cloned.1.call-done = bf16[2048,704]{1,0:T(8,128)(2,1)} async-done(((bf16[64,704]{1,0:T(8,128)(2,1)}), bf16[2048,704]{1,0:T(8,128)(2,1)}) %all-gather.4.cloned.1.call-update) | async-done | bytes 2883600 | tf_op jit(solution)/shard_map/all_gather | solution.py:11
  160.0 2.6 fusion.74
  162.6 3.2 constant_dynamic-update-slice_fusion.5
  166.5 1.6 fusion.93
  168.1 3.9 convolution_convert_fusion.1
  177.5 110.1 %all-reduce.7.cloned.1.call-done = (bf16[128,2048]{1,0:T(8,128)(2,1)}, bf16[128,2048]{1,0:T(8,128)(2,1)}) async-done(((bf16[128,2048]{1,0:T(8,128)(2,1)}, bf16[128,2048]{1,0:T(8,128)(2,1)}), (bf16[128,2048]{1,0:T(8,128)(2,1)}, bf16[128,2048]{1,0:T(8,128)(2,1)})) %all-reduce.7.cloned.1.call-update) | async-done | bytes 1048592 | tf_op jit(solution)/shard_map/psum | solution.py:45
  287.6 1.7 fusion.65
  289.3 1.7 fusion.48
  291.0 1.8 fusion.52
  295.9 1.7 fusion.82
  297.6 4.0 convolution_convert_fusion
  304.3 2.0 copy.40
  306.4 14.7 %all-to-all-start = ((bf16[128,32,64]{0,2,1:T(8,128)(2,1)}), bf16[128,32,64]{0,2,1:T(8,128)(2,1)}, u32[]{:S(2)}, u32[]{:S(2)}) async-start(bf16[128,32,64]{0,2,1:T(8,128)(2,1)} %bitcast.3), calls=%async_computation | async-start | bytes 1048576 | tf_op jit(solution)/shard_map/all_to_all | solution.py:150
  324.2 30.5 %all-to-all-done = bf16[128,32,64]{0,2,1:T(8,128)(2,1)} async-done(((bf16[128,32,64]{0,2,1:T(8,128)(2,1)}), bf16[128,32,64]{0,2,1:T(8,128)(2,1)}, u32[]{:S(2)}, u32[]{:S(2)}) %all-to-all-start) | async-done | bytes 524320 | tf_op jit(solution)/shard_map/all_to_all | solution.py:150
  354.7 4.0 all-to-all-start.2
  359.8 32.5 %all-to-all-done.2 = bf16[32,128,64]{1,2,0:T(8,128)(2,1)S(1)} async-done(((bf16[32,128,64]{1,2,0:T(8,128)(2,1)}), bf16[32,128,64]{1,2,0:T(8,128)(2,1)S(1)}, u32[]{:S(2)}, u32[]{:S(2)}) %all-to-all-start.2) | async-done | bytes 524320 | tf_op jit(solution)/shard_map/all_to_all | solution.py:138
  392.3 4.3 all-to-all-start.1
  397.7 23.6 %all-reduce.5.cloned.1.call-done = (bf16[128,2048]{1,0:T(8,128)(2,1)}, bf16[128,2048]{1,0:T(8,128)(2,1)}) async-done(((bf16[128,2048]{1,0:T(8,128)(2,1)}, bf16[128,2048]{1,0:T(8,128)(2,1)}), (bf16[128,2048]{1,0:T(8,128)(2,1)}, bf16[128,2048]{1,0:T(8,128)(2,1)})) %all-reduce.5.cloned.1.call-update) | async-done | bytes 1048592 | tf_op jit(solution)/shard_map/psum | solution.py:45
  422.6 7.5 %all-to-all-done.1 = bf16[128,32,64]{0,2,1:T(8,128)(2,1)S(1)} async-done(((bf16[128,32,64]{0,2,1:T(8,128)(2,1)}), bf16[128,32,64]{0,2,1:T(8,128)(2,1)S(1)}, u32[]{:S(2)}, u32[]{:S(2)}) %all-to-all-start.1) | async-done | bytes 524320 | tf_op jit(solution)/shard_map/all_to_all | solution.py:151
  430.2 6.9 %all-to-all-start.3 = ((bf16[128,32,64]{0,2,1:T(8,128)(2,1)}), bf16[128,32,64]{0,2,1:T(8,128)(2,1)S(1)}, u32[]{:S(2)}, u32[]{:S(2)}) async-start(bf16[128,32,64]{0,2,1:T(8,128)(2,1)} %bitcast.39), calls=%async_computation.3 | async-start | bytes 1048576 | tf_op jit(solution)/shard_map/all_to_all | solution.py:146
  437.1 2.7 fusion.59
  439.8 98.8 %all-gather.8.cloned.1.call-done = bf16[4096,1056]{0,1:T(8,128)(2,1)} async-done(((bf16[128,1056]{0,1:T(8,128)(2,1)}), bf16[4096,1056]{0,1:T(8,128)(2,1)}) %all-gather.8.cloned.1.call-update) | async-done | bytes 8650768 | tf_op jit(solution)/shard_map/all_gather | solution.py:11
  538.7 2.8 fusion.23
  541.4 2.8 fusion.26
  544.2 2.6 fusion.35
  546.8 2.6 fusion.38
  549.4 2.6 fusion.32
  552.0 2.6 fusion.44
  (107 shorter events, 23.6 us)
Async XLA Ops:
  7.2 80.3 %all-gather.6.cloned.1.call-start = ((), (), s32[]{:S(2)}) async-start(), calls=%async_computation.5 | async-start | bytes 1622016 | tf_op jit(solution)/shard_map/all_gather | solution.py:22
  8.7 151.3 %all-gather.4.cloned.1.call-start = ((), (), s32[]{:S(2)}) async-start(), calls=%async_computation.4 | async-start | bytes 3244032 | tf_op jit(solution)/shard_map/all_gather | solution.py:11
  10.4 277.3 %all-reduce.7.cloned.1.call-start = ((), (), s32[]{:S(2)}) async-start(), calls=%async_computation.8 | async-start | bytes 2097152 | tf_op jit(solution)/shard_map/psum | solution.py:45
  16.1 150.4 %copy-start.12 = (f32[2048]{0:T(1024)S(1)}, f32[2048]{0:T(1024)}, u32[]{:S(2)}) copy-start(f32[2048]{0:T(1024)} %param.22) | copy-start | bytes 24580
  160.0 6.5 %copy-start = (bf16[2048,704]{1,0:T(8,128)(2,1)S(1)}, bf16[2048,704]{1,0:T(8,128)(2,1)}, u32[]{:S(2)}) copy-start(bf16[2048,704]{1,0:T(8,128)(2,1)} %all-gather.4.cloned.1.call-done) | copy-start | bytes 8650756
  174.1 115.2 %copy-start.11 = (f32[2048]{0:T(1024)S(1)}, f32[2048]{0:T(1024)}, u32[]{:S(2)}) copy-start(f32[2048]{0:T(1024)} %param.23) | copy-start | bytes 24580
  174.1 247.1 %all-reduce.5.cloned.1.call-start = ((), (), s32[]{:S(2)}) async-start(), calls=%async_computation.7 | async-start | bytes 2097152 | tf_op jit(solution)/shard_map/psum | solution.py:45
  175.6 0.9 copy-start.5
  287.6 6.0 %copy-start.10 = (bf16[2048,352]{1,0:T(8,128)(2,1)S(1)}, bf16[2048,352]{1,0:T(8,128)(2,1)}, u32[]{:S(2)}) copy-start(bf16[2048,352]{1,0:T(8,128)(2,1)} %all-gather.6.cloned.1.call-done) | copy-start | bytes 4325380
  287.6 6.5 %copy-start.6 = (bf16[128,2048]{1,0:T(8,128)(2,1)S(1)}, bf16[128,2048]{1,0:T(8,128)(2,1)}, u32[]{:S(2)}) copy-start(bf16[128,2048]{1,0:T(8,128)(2,1)} %copy-done.5) | copy-start | bytes 1572868
  289.3 6.6 %copy-start.8 = (bf16[128,2048]{1,0:T(8,128)(2,1)}, bf16[128,2048]{1,0:T(8,128)(2,1)S(1)}, u32[]{:S(2)}) copy-start(bf16[128,2048]{1,0:T(8,128)(2,1)S(1)} %get-tuple-element.22) | copy-start | bytes 1572868
  292.8 0.8 copy-start.3
  303.6 17.5 %copy-start.1 = (bf16[128,2048]{1,0:T(8,128)(2,1)S(1)}, bf16[128,2048]{1,0:T(8,128)(2,1)}, u32[]{:S(2)}) copy-start(bf16[128,2048]{1,0:T(8,128)(2,1)} %fusion.47) | copy-start | bytes 1572868
  303.6 235.0 %all-gather.8.cloned.1.call-start = ((), (), s32[]{:S(2)}) async-start(), calls=%async_computation.6 | async-start | bytes 8921088 | tf_op jit(solution)/shard_map/all_gather | solution.py:11
  306.4 52.4 %copy-start.4 = (bf16[128,2048]{1,0:T(8,128)(2,1)S(1)}, bf16[128,2048]{1,0:T(8,128)(2,1)}, u32[]{:S(2)}) copy-start(bf16[128,2048]{1,0:T(8,128)(2,1)} %copy-done.3) | copy-start | bytes 1572868
  306.4 48.3 %all-to-all-start = ((bf16[128,32,64]{0,2,1:T(8,128)(2,1)}), bf16[128,32,64]{0,2,1:T(8,128)(2,1)}, u32[]{:S(2)}, u32[]{:S(2)}) async-start(bf16[128,32,64]{0,2,1:T(8,128)(2,1)} %bitcast.3), calls=%async_computation | async-start | bytes 1048576 | tf_op jit(solution)/shard_map/all_to_all | solution.py:150
  321.6 75.0 %copy-start.7 = (bf16[128,2048]{1,0:T(8,128)(2,1)S(1)}, bf16[128,2048]{1,0:T(8,128)(2,1)}, u32[]{:S(2)}) copy-start(bf16[128,2048]{1,0:T(8,128)(2,1)} %param.21) | copy-start | bytes 1572868
  322.6 98.6 %copy-start.2 = (bf16[128,2048]{1,0:T(8,128)(2,1)S(1)}, bf16[128,2048]{1,0:T(8,128)(2,1)}, u32[]{:S(2)}) copy-start(bf16[128,2048]{1,0:T(8,128)(2,1)} %param.19) | copy-start | bytes 1572868
  324.2 112.8 %copy-start.9 = (bf16[128,2048]{1,0:T(8,128)(2,1)S(1)}, bf16[128,2048]{1,0:T(8,128)(2,1)}, u32[]{:S(2)}) copy-start(bf16[128,2048]{1,0:T(8,128)(2,1)} %copy-done.8) | copy-start | bytes 1572868
  354.7 37.6 %all-to-all-start.2 = ((bf16[32,128,64]{1,2,0:T(8,128)(2,1)}), bf16[32,128,64]{1,2,0:T(8,128)(2,1)S(1)}, u32[]{:S(2)}, u32[]{:S(2)}) async-start(bf16[32,128,64]{1,2,0:T(8,128)(2,1)} %copy.44), calls=%async_computation.2 | async-start | bytes 1048576 | tf_op jit(solution)/shard_map/all_to_all | solution.py:138
  392.3 37.9 %all-to-all-start.1 = ((bf16[128,32,64]{0,2,1:T(8,128)(2,1)}), bf16[128,32,64]{0,2,1:T(8,128)(2,1)S(1)}, u32[]{:S(2)}, u32[]{:S(2)}) async-start(bf16[128,32,64]{0,2,1:T(8,128)(2,1)} %bitcast.5), calls=%async_computation.1 | async-start | bytes 1048576 | tf_op jit(solution)/shard_map/all_to_all | solution.py:151
  397.6 141.0 %copy-start.13 = (f32[64,176]{1,0:T(8,128)S(1)}, f32[64,176]{1,0:T(8,128)}, u32[]{:S(2)}) copy-start(f32[64,176]{1,0:T(8,128)} %param.30) | copy-start | bytes 135172
  430.2 121.8 %all-to-all-start.3 = ((bf16[128,32,64]{0,2,1:T(8,128)(2,1)}), bf16[128,32,64]{0,2,1:T(8,128)(2,1)S(1)}, u32[]{:S(2)}, u32[]{:S(2)}) async-start(bf16[128,32,64]{0,2,1:T(8,128)(2,1)} %bitcast.39), calls=%async_computation.3 | async-start | bytes 1048576 | tf_op jit(solution)/shard_map/all_to_all | solution.py:146
  437.0 104.4 %copy-start.14 = (f32[64,176]{1,0:T(8,128)S(1)}, f32[64,176]{1,0:T(8,128)}, u32[]{:S(2)}) copy-start(f32[64,176]{1,0:T(8,128)} %param.31) | copy-start | bytes 135172
  439.8 104.4 %copy-start.15 = (f32[64,176]{1,0:T(8,128)S(1)}, f32[64,176]{1,0:T(8,128)}, u32[]{:S(2)}) copy-start(f32[64,176]{1,0:T(8,128)} %param.33) | copy-start | bytes 135172
  439.8 107.0 %copy-start.16 = (f32[64,176]{1,0:T(8,128)S(1)}, f32[64,176]{1,0:T(8,128)}, u32[]{:S(2)}) copy-start(f32[64,176]{1,0:T(8,128)} %param.34) | copy-start | bytes 135172
  541.4 8.0 %copy-start.17 = (f32[176,64]{0,1:T(8,128)S(1)}, f32[176,64]{0,1:T(8,128)}, u32[]{:S(2)}) copy-start(f32[176,64]{0,1:T(8,128)} %param.32) | copy-start | bytes 135172
  546.8 5.2 copy-start.18
Sparse Core Ops, SparseCore 0:
  10.7 76.7 all-gather.5
  90.1 69.8 all-gather.3
  174.3 113.3 all-reduce.6
  303.7 117.4 all-reduce.4
  423.1 115.4 all-gather.7
